TPU v7x, 32 devices: a whole 2x2x4 slice. The times are simulated.
32 devices in a mesh: sp: 4 (over y, x), tp: 8 (over z, core).
Axes of the slice: x: 2, y: 2, z: 4, core: 2. Of those that a mesh axis runs over, the one named last changes fastest.
Arguments:
- stream: bfloat16 [8, 1536, 2048], P('tp', 'sp'), may hold values from -80 to 80
- norm_gain: float32 [2048], replicated, may hold values from 0.1 to 1.9
- w_lin: bfloat16 [1024, 2048], P('tp'), may hold values from -0.125 to 0.125
- w_gate: bfloat16 [1024, 2048], P('tp'), may hold values from -0.125 to 0.125
- conv_taps: bfloat16 [31, 1024], replicated, may hold values from -3 to 3
- conv_bias: float32 [1024], replicated, may hold values from -3 to 3
- ln_gain: float32 [1024], replicated, may hold values from 0.1 to 1.9
- ln_shift: float32 [1024], replicated, may hold values from -3 to 3
- w_proj: bfloat16 [1024, 2048], P('tp'), may hold values from -0.1875 to 0.1875
Outputs:
- result_stream: bfloat16 [8, 1536, 2048], P('tp', 'sp')
All inputs are finite; a program needn't handle non-finite values.
Results may differ from a plain program's by a relative error of at most 0.0024.
Values may be sent and summed in bfloat16 or wider, within the bound.
A program may use at most 64 MiB of HBM per device.

v0:
```python
import functools

import jax
import jax.numpy as jnp
from jax import lax
from jax.experimental import pallas as pl
from jax.experimental.pallas import tpu as pltpu
from jax.sharding import PartitionSpec as P

EPS = 1e-06
HALO = 32
F32 = jnp.float32
BF16 = jnp.bfloat16
MESH = pl.DeviceIdType.MESH


def kernel(
    nsp, nz, kw,
    x_any, gain_any, wl_ref, wg_ref, wp_ref, taps_any, bias_any, lng_any, lnb_any,
    out_any,
    x_ref, out_ref, gain_ref, taps_ref, bias_ref, lng_ref, lnb_ref, held, xh, normed, mix, conv, act, taps,
    local_sem, out_sem, halo_sem, z_recv, x_recv, y_recv, d_recv, up_send, dn_send, x_send, y_send, d_send, dp_recv, dp_send,
):
    rows, width = x_ref.shape
    block = held.shape[2]
    shard = block // 2
    lanes = min(128, block)
    strips = block // lanes
    quarter = width // 4
    half = quarter // 2
    p, tp = lax.axis_index("sp"), lax.axis_index("tp")
    z, c = tp // 2, tp % 2
    q = p % 4
    low, high = q % 2, q // 2
    beside = (p + 1 - 2 * low, tp)
    across = (p + 2 - 4 * high, tp)
    twin = (p, z * 2 + 1 - c)
    above = (p, tp + 2)
    below = (p, tp - 2)
    parity = (low + high) % 2
    has_up, has_dn = z < nz - 1, z > 0
    has_next, has_prev = p < nsp - 1, p > 0
    qx, qy, qd = q + 1 - 2 * low, q + 2 - 4 * high, 3 - q

    def cols(start, size):
        return pl.ds(pl.multiple_of(start, 128), size)

    def at(kind, src, core, start, size):
        return held.at[kind, src, pl.ds(pl.multiple_of(core * shard, 16), shard), cols(start, size)]

    def send(piece, ssem, rsem, target):
        return pltpu.make_async_remote_copy(
            src_ref=piece, dst_ref=piece, send_sem=ssem, recv_sem=rsem, device_id=target, device_id_type=MESH
        )

    def final(kind):
        return isinstance(kind, int) and kind == 2

    def z_piece(kind, src, i):
        if not final(kind):
            return at(kind, src, c, q * quarter, quarter)
        return at(kind, src, c, (parity * 2 + i) * quarter, quarter)

    def z_copy(kind, src, i, up):
        return send(
            z_piece(kind, src, i), (up_send if up else dn_send).at[kind, src, i], z_recv.at[kind, src, i],
            above if up else below,
        )

    def z_pieces(kind):
        return 2 if final(kind) else 1

    def x_copy(kind, src, i, incoming):
        if final(kind):
            piece = at(2, src, c, ((1 - parity if incoming else parity) * 2) * quarter, quarter)
        elif i == 0:
            piece = at(kind, src, c, (qx if incoming else q) * quarter, quarter)
        else:
            piece = at(kind, src, c, (qd if incoming else qy) * quarter, half)
        return send(piece, x_send.at[kind, src, i], x_recv.at[kind, src, i], beside)

    def y_copy(kind, src, i, incoming):
        if final(kind):
            piece = at(2, src, c, ((1 - parity if incoming else parity) * 2 + 1) * quarter, quarter)
        elif i == 0:
            piece = at(kind, src, c, (qy if incoming else q) * quarter, quarter)
        else:
            piece = at(kind, src, c, (qd if incoming else qx) * quarter + half, half)
        return send(piece, y_send.at[kind, src, i], y_recv.at[kind, src, i], across)

    def d_copy(kind, src, core):
        return send(at(kind, src, core, 0, width), d_send.at[kind, src], d_recv.at[kind, src], twin)

    def d_piece(kind, src, start, size):
        return send(at(kind, src, c, start, size), d_send.at[kind, src], d_recv.at[kind, src], twin)

    def p_cols(slot):
        return ((parity + slot // 2) % 2 * 2 + slot % 2) * quarter

    def p_copy(src, slot, core):
        return send(at(2, src, core, p_cols(slot), quarter), dp_send.at[src, slot], dp_recv.at[src, slot], twin)

    def halo_copy():
        return pltpu.make_async_remote_copy(
            src_ref=x_ref.at[pl.ds(rows - HALO, HALO)], dst_ref=xh, send_sem=halo_sem.at[0],
            recv_sem=halo_sem.at[1], device_id=(p + 1, tp), device_id_type=MESH,
        )

    mine = [
        pltpu.make_async_copy(ref, at(kind, z, c, 0, width), local_sem.at[kind])
        for kind, ref in enumerate((wl_ref, wg_ref, wp_ref))
    ]
    stream_in = pltpu.make_async_copy(x_any, x_ref, local_sem.at[3])
    mine[0].start()
    stream_in.start()
    mine[1].start()
    small = [
        pltpu.make_async_copy(ref, there, local_sem.at[4 + i])
        for i, (ref, there) in enumerate((
            (gain_any, gain_ref), (taps_any, taps_ref), (bias_any, bias_ref), (lng_any, lng_ref), (lnb_any, lnb_ref),
        ))
    ]
    for copy in small:
        copy.start()
    mine[2].start()

    barrier = pltpu.get_barrier_semaphore()
    for target in (beside, across, twin):
        pl.semaphore_signal(barrier, inc=1, device_id=target, device_id_type=MESH)
    for there, target in (
        (has_up, above), (has_dn, below), (has_next, (p + 1, tp)), (has_prev, (p - 1, tp)),
    ):
        @pl.when(there)
        def _():
            pl.semaphore_signal(barrier, inc=1, device_id=target, device_id_type=MESH)

    one = lambda there: jnp.where(there, 1, 0)
    pl.semaphore_wait(barrier, 3 + one(has_up) + one(has_dn) + one(has_next) + one(has_prev))

    def start_own(kind):
        for i in range(z_pieces(kind)):
            @pl.when(has_up)
            def _():
                z_copy(kind, z, i, True).start()

            @pl.when(has_dn)
            def _():
                z_copy(kind, z, i, False).start()

    mine[0].wait()
    start_own(0)
    mine[1].wait()
    start_own(1)
    stream_in.wait()

    @pl.when(has_next)
    def _():
        halo_copy().start()

    d_copy(0, z, c).start()
    d_copy(1, z, c).start()
    mine[2].wait()
    for slot in range(4):
        p_copy(z, slot, c).start()

    @pl.when(has_up & (z == 0))
    def _():
        for i in range(2):
            z_copy(2, z, i, True).start()

    @pl.when(has_dn & (z == nz - 1))
    def _():
        for i in range(2):
            z_copy(2, z, i, False).start()

    def each(t, body):
        for sign in (-1, 1):
            src = z + sign * t

            @pl.when((src >= 0) & (src < nz))
            def _():
                body(src, sign)

    def pass_on(kind, src, sign, i):
        z_copy(kind, src, i, True).wait_recv()
        if sign < 0:
            @pl.when(has_up)
            def _():
                z_copy(kind, src, i, True).start()
        else:
            @pl.when(has_dn)
            def _():
                z_copy(kind, src, i, False).start()

    def relay(kind):
        def body(src, sign):
            pass_on(kind, src, sign, 0)
            x_copy(kind, src, 0, False).start()
            y_copy(kind, src, 0, False).start()
            d_piece(kind, src, q * quarter, quarter).start()

        return body

    def onward(i):
        def body(src, sign):
            pass_on(2, src, sign, i)
            p_copy(src, i, c).start()

        return body

    def sideways(i):
        def body(src, sign):
            @pl.when(i == 0)
            def _():
                x_copy(2, src, 0, False).start()

            @pl.when(i == 1)
            def _():
                y_copy(2, src, 0, False).start()

        return body

    def diagonal(kind):
        def body(src, sign):
            x_copy(kind, src, 0, True).wait_recv()
            y_copy(kind, src, 1, False).start()
            d_piece(kind, src, qx * quarter, quarter).start()
            y_copy(kind, src, 0, True).wait_recv()
            x_copy(kind, src, 1, False).start()
            d_piece(kind, src, qy * quarter, quarter).start()

        return body

    def finish(kind):
        def body(src, sign):
            x_copy(kind, src, 1, True).wait_recv()
            d_piece(kind, src, qd * quarter, half).start()
            y_copy(kind, src, 1, True).wait_recv()
            d_piece(kind, src, qd * quarter + half, half).start()

        return body

    def arrived(src, sign):
        x_copy(2, src, 0, True).wait_recv()
        p_copy(src, 2, c).start()
        y_copy(2, src, 0, True).wait_recv()
        p_copy(src, 3, c).start()

    def norm_into(ref, base, count):
        @pl.loop(0, count // 16)
        def _(r):
            full = ref[pl.ds(pl.multiple_of(r * 16, 16), 16), :].astype(F32)
            scale = lax.rsqrt(jnp.mean(full * full, axis=1, keepdims=True) + EPS)
            normed[pl.ds(pl.multiple_of(base + r * 16, 16), 16), :] = (full * scale * gain_ref[...]).astype(BF16)

    for copy in small:
        copy.wait()
    norm_into(x_ref, HALO, rows)
    for i in range(nz):
        taps[i, 0:kw] = taps_ref[:, i * block:(i + 1) * block].astype(F32)
        taps[i, kw:kw + 1] = bias_ref[:, i * block:(i + 1) * block]

    @pl.when(has_prev)
    def _():
        halo_copy().wait_recv()

    @pl.when(jnp.logical_not(has_prev))
    def _():
        xh[...] = jnp.zeros_like(xh)

    norm_into(xh, 0, HALO)

    tile = 64
    lead = HALO - (kw - 1)
    nt = (((1,), (1,)), ((), ()))

    def on_planes(t, body):
        def one_side(side, carry):
            src = z + (2 * side - 1) * t
            valid = (src >= 0) & (src < nz) & ((t > 0) | (side == 0))

            @pl.when(valid)
            def _():
                body(side, src)

            return carry

        lax.fori_loop(0, 2, one_side, 0)

    def gate(t):
        def body(side, src):
            d_copy(0, src, 1 - c).wait_recv()
            d_copy(1, src, 1 - c).wait_recv()
            linear = lax.dot_general(normed[...], held[0, src], nt, preferred_element_type=F32)
            gating = lax.dot_general(normed[...], held[1, src], nt, preferred_element_type=F32)
            mixed = (linear * jax.nn.sigmoid(gating)).astype(BF16).astype(F32)
            for s in range(strips):
                mix[side, s, 0:HALO + rows] = mixed[:, s * lanes:(s + 1) * lanes]

        on_planes(t, body)

    def convolve(t):
        def body(side, src):
            @pl.loop(0, rows // tile)
            def _(r):
                base = pl.multiple_of(r * tile, tile)
                for s in range(strips):
                    lane = slice(s * lanes, (s + 1) * lanes)
                    total = jnp.broadcast_to(taps[src, kw:kw + 1, lane], (tile, lanes))
                    for b in range(8):
                        slab = mix[side, s, pl.ds(base + b, tile + HALO), :]
                        for a in range(HALO // 8 + 1):
                            tap = 8 * a + b - lead
                            if 0 <= tap < kw:
                                total = total + taps[src, tap:tap + 1, lane] * slab[8 * a:8 * a + tile]
                    conv[src, pl.ds(base, tile), lane] = total

        on_planes(t, body)

    slots = 2 * (nz - 1)

    @pl.loop(0, slots)
    def _(m):
        each(1 + m // 2, relay(m % 2))

        @pl.when((m % 2 == 1) & (1 + m // 2 == z) & has_up)
        def _():
            for i in range(2):
                z_copy(2, z, i, True).start()

        @pl.when((m % 2 == 1) & (1 + m // 2 == nz - 1 - z) & has_dn)
        def _():
            for i in range(2):
                z_copy(2, z, i, False).start()

        @pl.when(m >= 2)
        def _():
            each(m // 2, diagonal(m % 2))

        @pl.when(m == 0)
        def _():
            gate(0)

        @pl.when(m == 1)
        def _():
            convolve(0)

    @pl.loop(0, slots)
    def _(m):
        t, i = 1 + m // 2, m % 2
        each(t, onward(i))

        @pl.when(m < 2)
        def _():
            each(nz - 1, diagonal(i))

        @pl.when(m == 1)
        def _():
            each(1, sideways(0))
            each(1, sideways(1))

        @pl.when(m >= 2)
        def _():
            each(t, sideways(i))

        @pl.when(i == 0)
        def _():
            @pl.when(m > 0)
            def _():
                convolve(t - 1)

            each(t, finish(0))
            each(t, finish(1))

        @pl.when(i == 1)
        def _():
            gate(t)

    convolve(nz - 1)

    channels = nz * block

    @pl.loop(0, rows // 16)
    def _(r):
        here = pl.ds(pl.multiple_of(r * 16, 16), 16)
        parts = [conv[i, here, :] for i in range(nz)]
        mean = sum(jnp.sum(v, axis=1, keepdims=True) for v in parts) / channels
        meansq = sum(jnp.sum(v * v, axis=1, keepdims=True) for v in parts) / channels
        scale = lax.rsqrt(meansq - mean * mean + EPS)
        for i, v in enumerate(parts):
            lane = slice(i * block, (i + 1) * block)
            u = (v - mean) * scale * lng_ref[:, lane] + lnb_ref[:, lane]
            act[i, here, :] = (u * jax.nn.sigmoid(u)).astype(BF16)

    def out_copy(n):
        here = cols(p_cols(n), quarter)
        return pltpu.make_async_copy(out_ref.at[:, here], out_any.at[:, here], out_sem.at[n])

    @pl.loop(0, 4)
    def _(n):
        @pl.when(n == 2)
        def _():
            @pl.loop(1, nz)
            def _(t):
                each(t, arrived)

        @pl.loop(0, nz)
        def _(src):
            p_copy(src, n, 1 - c).wait_recv()

        here = cols(p_cols(n), quarter)
        total = x_ref[:, here].astype(F32)
        for i in range(nz):
            total = total + jnp.dot(act[i], held[2, i, :, here], preferred_element_type=F32)
        out_ref[:, here] = total.astype(BF16)
        out_copy(n).start()

    for n in range(4):
        out_copy(n).wait()

    @pl.when(has_next)
    def _():
        halo_copy().wait_send()

    for kind in range(3):
        @pl.loop(0, nz)
        def _(src):
            if final(kind):
                for slot in range(4):
                    p_copy(src, slot, c).wait_send()
            else:
                d_copy(kind, src, c).wait_send()

            @pl.when(src != z)
            def _():
                for i in range(2 if kind < 2 else 1):
                    x_copy(kind, src, i, False).wait_send()
                    y_copy(kind, src, i, False).wait_send()

            for i in range(z_pieces(kind)):
                @pl.when((src <= z) & has_up)
                def _():
                    z_copy(kind, src, i, True).wait_send()

                @pl.when((src >= z) & has_dn)
                def _():
                    z_copy(kind, src, i, False).wait_send()


def local(nsp, ntp, stream, norm_gain, w_lin, w_gate, conv_taps, conv_bias, ln_gain, ln_shift, w_proj):
    _, rows, width = stream.shape
    kw, channels = conv_taps.shape
    nz = ntp // 2
    block = channels // nz
    lanes = min(128, block)
    kept = pl.BlockSpec(memory_space=pltpu.HBM)
    dma = pltpu.SemaphoreType.DMA
    out = pl.pallas_call(
        functools.partial(kernel, nsp, nz, kw),
        out_shape=jax.ShapeDtypeStruct((rows, width), BF16),
        in_specs=[kept] * 9,
        out_specs=pl.BlockSpec(memory_space=pl.ANY),
        scratch_shapes=[
            pltpu.VMEM((rows, width), BF16),
            pltpu.VMEM((rows, width), BF16),
            pltpu.VMEM((1, width), F32),
            pltpu.VMEM((kw, channels), BF16),
            pltpu.VMEM((1, channels), F32),
            pltpu.VMEM((1, channels), F32),
            pltpu.VMEM((1, channels), F32),
            pltpu.VMEM((3, nz, block, width), BF16),
            pltpu.VMEM((HALO, width), BF16),
            pltpu.VMEM((HALO + rows, width), BF16),
            pltpu.VMEM((2, block // lanes, HALO + rows + 8, lanes), F32),
            pltpu.VMEM((nz, rows, block), F32),
            pltpu.VMEM((nz, rows, block), BF16),
            pltpu.VMEM((nz, kw + 1, block), F32),
            dma((9,)), dma((4,)), dma((2,)),
            dma((3, nz, 2)), dma((3, nz, 2)), dma((3, nz, 2)), dma((3, nz)),
            dma((3, nz, 2)), dma((3, nz, 2)), dma((3, nz, 2)), dma((3, nz, 2)), dma((3, nz)), dma((nz, 4)), dma((nz, 4)),
        ],
        compiler_params=pltpu.CompilerParams(
            collective_id=0, has_side_effects=True, vmem_limit_bytes=60 * 1024 * 1024
        ),
    )(
        stream[0], norm_gain[None], w_lin, w_gate, w_proj, conv_taps,
        conv_bias[None], ln_gain[None], ln_shift[None],
    )
    return out[None]


def solution(mesh):
    placed = (
        P("tp", "sp", None), P(), P("tp", None), P("tp", None), P(), P(), P(), P(), P("tp", None),
    )
    return jax.shard_map(
        functools.partial(local, mesh.shape["sp"], mesh.shape["tp"]),
        mesh=mesh, in_specs=placed, out_specs=P("tp", "sp", None), check_vma=False,
    )
```

profile of v0, /device:TPU:0, one launch (start us, length us, event | category | flops | bytes accessed | tf_op | source)
XLA Modules:
  0.0 59.8 jit_solution(10255006705198978347)
XLA Ops:
  0.0 57.0 %shard_map.91 = bf16[384,2048]{1,0:T(8,128)(2,1)} custom-call(bf16[384,2048]{1,0:T(8,128)(2,1)} %bitcast.7, f32[1,2048]{1,0:T(1,128)} %bitcast.8, bf16[128,2048]{1,0:T(8,128)(2,1)} %wl_ref.1, bf16[128,2048]{1,0:T(8,128)(2,1)} %wg_ref.1, bf16[128,2048]{1,0:T(8,128)(2,1)} %wp_ref.1, bf16[31,1024]{1,0:T(8,128)(2,1)} %taps_any.1, f32[1,1024]{1,0:T(1,128)} %bitcast.9, ...), custom_call_target="tpu_custom_call" | custom-call | tf_op jit(solution)/shard_map/pallas_call | solution.py:458
  57.0 2.7 %copy.11 = bf16[1,384,2048]{2,1,0:T(8,128)(2,1)} copy(bf16[1,384,2048]{2,1,0:T(8,128)(2,1)} %bitcast.6) | data formatting | bytes 3145728
where the time goes:
time: 59.9 us; the launch traced here: 59.8 us
  Pallas kernels  57 us (95%)
  local copies, waits for them, and re-layouts  2.73 us (5%)
    pallas_call x1, Pallas kernels, local(): pl.pallas_call(functools.partial(kernel, nsp, nz, kw), out_shape=jax.Shap...  57 us
    unnamed x1, local copies, waits for them, and re-layouts  2.73 us

commit v1 on v0

--- a/solution.py
+++ b/solution.py
@@ -17,9 +17,9 @@
 def kernel(
     nsp, nz, kw,
     x_any, gain_any, wl_ref, wg_ref, wp_ref, taps_any, bias_any, lng_any, lnb_any,
-    out_any,
-    x_ref, out_ref, gain_ref, taps_ref, bias_ref, lng_ref, lnb_ref, held, xh, normed, mix, conv, act, taps,
-    local_sem, out_sem, halo_sem, z_recv, x_recv, y_recv, d_recv, up_send, dn_send, x_send, y_send, d_send, dp_recv, dp_send,
+    out_ref,
+    x_ref, gain_ref, taps_ref, bias_ref, lng_ref, lnb_ref, held, xh, normed, mix, conv, act, taps,
+    local_sem, halo_sem, z_recv, x_recv, y_recv, d_recv, up_send, dn_send, x_send, y_send, d_send, dp_recv, dp_send,
 ):
     rows, width = x_ref.shape
     block = held.shape[2]
@@ -392,10 +392,6 @@
             u = (v - mean) * scale * lng_ref[:, lane] + lnb_ref[:, lane]
             act[i, here, :] = (u * jax.nn.sigmoid(u)).astype(BF16)
 
-    def out_copy(n):
-        here = cols(p_cols(n), quarter)
-        return pltpu.make_async_copy(out_ref.at[:, here], out_any.at[:, here], out_sem.at[n])
-
     @pl.loop(0, 4)
     def _(n):
         @pl.when(n == 2)
@@ -413,10 +409,6 @@
         for i in range(nz):
             total = total + jnp.dot(act[i], held[2, i, :, here], preferred_element_type=F32)
         out_ref[:, here] = total.astype(BF16)
-        out_copy(n).start()
-
-    for n in range(4):
-        out_copy(n).wait()
 
     @pl.when(has_next)
     def _():
@@ -457,11 +449,10 @@
     dma = pltpu.SemaphoreType.DMA
     out = pl.pallas_call(
         functools.partial(kernel, nsp, nz, kw),
-        out_shape=jax.ShapeDtypeStruct((rows, width), BF16),
+        out_shape=pltpu.VMEM((rows, width), BF16),
         in_specs=[kept] * 9,
-        out_specs=pl.BlockSpec(memory_space=pl.ANY),
+        out_specs=pl.BlockSpec(memory_space=pltpu.VMEM),
         scratch_shapes=[
-            pltpu.VMEM((rows, width), BF16),
             pltpu.VMEM((rows, width), BF16),
             pltpu.VMEM((1, width), F32),
             pltpu.VMEM((kw, channels), BF16),
@@ -475,7 +466,7 @@
             pltpu.VMEM((nz, rows, block), F32),
             pltpu.VMEM((nz, rows, block), BF16),
             pltpu.VMEM((nz, kw + 1, block), F32),
-            dma((9,)), dma((4,)), dma((2,)),
+            dma((9,)), dma((2,)),
             dma((3, nz, 2)), dma((3, nz, 2)), dma((3, nz, 2)), dma((3, nz)),
             dma((3, nz, 2)), dma((3, nz, 2)), dma((3, nz, 2)), dma((3, nz, 2)), dma((3, nz)), dma((nz, 4)), dma((nz, 4)),
         ],

time: 59.9 us -> 57.5 us (0.960)
  local copies, waits for them, and re-layouts: 2.73 us -> 1.15 us
  Pallas kernels: 57 us -> 56.2 us
    unnamed x1, local copies, waits for them, and re-layouts: 2.73 us -> 1.15 us
    pallas_call x1, Pallas kernels: 57 us -> 56.2 us  [local(): pl.pallas_call(functools.partial(kernel, nsp, nz, kw), out_shape=pltpu.VM...]
where the time goes in v1:
time: 57.5 us; the launch traced here: 57.4 us
  Pallas kernels  56.2 us (98%)
  local copies, waits for them, and re-layouts  1.15 us (2%)
    pallas_call x1, Pallas kernels, local(): pl.pallas_call(functools.partial(kernel, nsp, nz, kw), out_shape=pltpu.VM...  56.2 us

profile of v1, /device:TPU:0, one launch (start us, length us, event | category | flops | bytes accessed | tf_op | source)
XLA Modules:
  0.0 57.4 jit_solution(10661595160272142941)
XLA Ops:
  0.0 56.2 %shard_map.91 = bf16[384,2048]{1,0:T(8,128)(2,1)S(1)} custom-call(bf16[384,2048]{1,0:T(8,128)(2,1)} %bitcast.7, f32[1,2048]{1,0:T(1,128)} %bitcast.8, bf16[128,2048]{1,0:T(8,128)(2,1)} %wl_ref.1, bf16[128,2048]{1,0:T(8,128)(2,1)} %wg_ref.1, bf16[128,2048]{1,0:T(8,128)(2,1)} %wp_ref.1, bf16[31,1024]{1,0:T(8,128)(2,1)} %taps_any.1, f32[1,1024]{1,0:T(1,128)} %bitcast.9, ...), custom_call_target="tpu_custom_call" | custom-call | tf_op jit(solution)/shard_map/pallas_call | solution.py:450
  56.2 1.1 %copy.11 = bf16[1,384,2048]{2,1,0:T(8,128)(2,1)} copy(bf16[1,384,2048]{2,1,0:T(8,128)(2,1)S(1)} %bitcast.6) | data formatting | bytes 3145728

commit v2 on v1

--- a/solution.py
+++ b/solution.py
@@ -18,8 +18,8 @@
     nsp, nz, kw,
     x_any, gain_any, wl_ref, wg_ref, wp_ref, taps_any, bias_any, lng_any, lnb_any,
     out_ref,
-    x_ref, gain_ref, taps_ref, bias_ref, lng_ref, lnb_ref, held, xh, normed, mix, conv, act, taps,
-    local_sem, halo_sem, z_recv, x_recv, y_recv, d_recv, up_send, dn_send, x_send, y_send, d_send, dp_recv, dp_send,
+    x_ref, gain_ref, taps_ref, bias_ref, lng_ref, lnb_ref, held, xh, normed, mix, conv, act, taps, acc,
+    local_sem, halo_sem, z_recv, x_recv, y_recv, d_recv, up_send, dn_send, x_send, y_send, d_send, dp_recv,
 ):
     rows, width = x_ref.shape
     block = held.shape[2]
@@ -37,7 +37,6 @@
     twin = (p, z * 2 + 1 - c)
     above = (p, tp + 2)
     below = (p, tp - 2)
-    parity = (low + high) % 2
     has_up, has_dn = z < nz - 1, z > 0
     has_next, has_prev = p < nsp - 1, p > 0
     qx, qy, qd = q + 1 - 2 * low, q + 2 - 4 * high, 3 - q
@@ -53,52 +52,43 @@
             src_ref=piece, dst_ref=piece, send_sem=ssem, recv_sem=rsem, device_id=target, device_id_type=MESH
         )
 
-    def final(kind):
-        return isinstance(kind, int) and kind == 2
-
-    def z_piece(kind, src, i):
-        if not final(kind):
-            return at(kind, src, c, q * quarter, quarter)
-        return at(kind, src, c, (parity * 2 + i) * quarter, quarter)
+    def direct(kind, src):
+        return (kind == 2) | ((kind == 1) & ((src == 0) | (src == nz - 1)))
+
+    def full(kind, src):
+        return (kind == 0) & (((src == 0) & (z == 1)) | ((src == nz - 1) & (z == nz - 2)))
 
     def z_copy(kind, src, i, up):
         return send(
-            z_piece(kind, src, i), (up_send if up else dn_send).at[kind, src, i], z_recv.at[kind, src, i],
-            above if up else below,
+            at(kind, src, c, (q, qd, qx, qy)[i] * quarter, quarter),
+            (up_send if up else dn_send).at[kind, src, i], z_recv.at[kind, src, i], above if up else below,
         )
 
-    def z_pieces(kind):
-        return 2 if final(kind) else 1
-
     def x_copy(kind, src, i, incoming):
-        if final(kind):
-            piece = at(2, src, c, ((1 - parity if incoming else parity) * 2) * quarter, quarter)
-        elif i == 0:
+        if i == 0:
             piece = at(kind, src, c, (qx if incoming else q) * quarter, quarter)
         else:
             piece = at(kind, src, c, (qd if incoming else qy) * quarter, half)
         return send(piece, x_send.at[kind, src, i], x_recv.at[kind, src, i], beside)
 
     def y_copy(kind, src, i, incoming):
-        if final(kind):
-            piece = at(2, src, c, ((1 - parity if incoming else parity) * 2 + 1) * quarter, quarter)
-        elif i == 0:
+        if i == 0:
             piece = at(kind, src, c, (qy if incoming else q) * quarter, quarter)
         else:
             piece = at(kind, src, c, (qd if incoming else qx) * quarter + half, half)
         return send(piece, y_send.at[kind, src, i], y_recv.at[kind, src, i], across)
 
     def d_copy(kind, src, core):
-        return send(at(kind, src, core, 0, width), d_send.at[kind, src], d_recv.at[kind, src], twin)
+        return send(at(kind, src, core, 0, width), d_send, d_recv.at[kind, src], twin)
 
     def d_piece(kind, src, start, size):
-        return send(at(kind, src, c, start, size), d_send.at[kind, src], d_recv.at[kind, src], twin)
+        return send(at(kind, src, c, start, size), d_send, d_recv.at[kind, src], twin)
 
     def p_cols(slot):
-        return ((parity + slot // 2) % 2 * 2 + slot % 2) * quarter
+        return (q, qx, qy, qd)[slot] * quarter
 
     def p_copy(src, slot, core):
-        return send(at(2, src, core, p_cols(slot), quarter), dp_send.at[src, slot], dp_recv.at[src, slot], twin)
+        return send(at(2, src, core, p_cols(slot), quarter), d_send, dp_recv.at[src, slot], twin)
 
     def halo_copy():
         return pltpu.make_async_remote_copy(
@@ -137,20 +127,25 @@
     one = lambda there: jnp.where(there, 1, 0)
     pl.semaphore_wait(barrier, 3 + one(has_up) + one(has_dn) + one(has_next) + one(has_prev))
 
-    def start_own(kind):
-        for i in range(z_pieces(kind)):
-            @pl.when(has_up)
-            def _():
-                z_copy(kind, z, i, True).start()
-
-            @pl.when(has_dn)
-            def _():
-                z_copy(kind, z, i, False).start()
+    def start_own(kind, i, up):
+        @pl.when(has_up if up else has_dn)
+        def _():
+            z_copy(kind, z, i, up).start()
+
+    def start_ends(*pieces):
+        for up, there in ((True, has_up & (z == 0)), (False, has_dn & (z == nz - 1))):
+            @pl.when(there)
+            def _():
+                for kind, i in pieces:
+                    z_copy(kind, z, i, up).start()
 
     mine[0].wait()
-    start_own(0)
+    start_own(0, 0, True)
+    start_own(0, 0, False)
     mine[1].wait()
-    start_own(1)
+    start_own(1, 0, True)
+    start_own(1, 0, False)
+    start_ends((1, 1), (0, 1), (0, 2), (0, 3))
     stream_in.wait()
 
     @pl.when(has_next)
@@ -163,15 +158,7 @@
     for slot in range(4):
         p_copy(z, slot, c).start()
 
-    @pl.when(has_up & (z == 0))
-    def _():
-        for i in range(2):
-            z_copy(2, z, i, True).start()
-
-    @pl.when(has_dn & (z == nz - 1))
-    def _():
-        for i in range(2):
-            z_copy(2, z, i, False).start()
+    start_ends((2, 0), (2, 1))
 
     def each(t, body):
         for sign in (-1, 1):
@@ -192,59 +179,78 @@
             def _():
                 z_copy(kind, src, i, False).start()
 
+    def twin_piece(kind, src, slot):
+        if isinstance(kind, int) and kind == 2:
+            p_copy(src, slot, c).start()
+        else:
+            d_piece(kind, src, p_cols(slot), quarter).start()
+
+    def sideways(kind):
+        def body(src, sign):
+            @pl.when(jnp.logical_not(full(kind, src)))
+            def _():
+                x_copy(kind, src, 0, False).start()
+                y_copy(kind, src, 0, False).start()
+
+        return body
+
     def relay(kind):
         def body(src, sign):
             pass_on(kind, src, sign, 0)
-            x_copy(kind, src, 0, False).start()
-            y_copy(kind, src, 0, False).start()
-            d_piece(kind, src, q * quarter, quarter).start()
+            twin_piece(kind, src, 0)
 
         return body
 
-    def onward(i):
+    def relay_far(kind):
         def body(src, sign):
-            pass_on(2, src, sign, i)
-            p_copy(src, i, c).start()
-
-        return body
-
-    def sideways(i):
-        def body(src, sign):
-            @pl.when(i == 0)
-            def _():
-                x_copy(2, src, 0, False).start()
-
-            @pl.when(i == 1)
-            def _():
-                y_copy(2, src, 0, False).start()
+            @pl.when(direct(kind, src))
+            def _():
+                pass_on(kind, src, sign, 1)
+                twin_piece(kind, src, 3)
 
         return body
 
     def diagonal(kind):
         def body(src, sign):
-            x_copy(kind, src, 0, True).wait_recv()
-            y_copy(kind, src, 1, False).start()
-            d_piece(kind, src, qx * quarter, quarter).start()
-            y_copy(kind, src, 0, True).wait_recv()
-            x_copy(kind, src, 1, False).start()
-            d_piece(kind, src, qy * quarter, quarter).start()
+            more = jnp.logical_not(direct(kind, src))
+
+            @pl.when(jnp.logical_not(full(kind, src)))
+            def _():
+                x_copy(kind, src, 0, True).wait_recv()
+
+                @pl.when(more)
+                def _():
+                    y_copy(kind, src, 1, False).start()
+
+                twin_piece(kind, src, 1)
+                y_copy(kind, src, 0, True).wait_recv()
+
+                @pl.when(more)
+                def _():
+                    x_copy(kind, src, 1, False).start()
+
+                twin_piece(kind, src, 2)
 
         return body
 
     def finish(kind):
         def body(src, sign):
-            x_copy(kind, src, 1, True).wait_recv()
-            d_piece(kind, src, qd * quarter, half).start()
-            y_copy(kind, src, 1, True).wait_recv()
-            d_piece(kind, src, qd * quarter + half, half).start()
+            whole = full(kind, src)
+
+            @pl.when(jnp.logical_not(direct(kind, src) | whole))
+            def _():
+                x_copy(kind, src, 1, True).wait_recv()
+                d_piece(kind, src, qd * quarter, half).start()
+                y_copy(kind, src, 1, True).wait_recv()
+                d_piece(kind, src, qd * quarter + half, half).start()
+
+            @pl.when(whole)
+            def _():
+                for i, slot in ((1, 3), (2, 1), (3, 2)):
+                    z_copy(kind, src, i, True).wait_recv()
+                    twin_piece(kind, src, slot)
 
         return body
-
-    def arrived(src, sign):
-        x_copy(2, src, 0, True).wait_recv()
-        p_copy(src, 2, c).start()
-        y_copy(2, src, 0, True).wait_recv()
-        p_copy(src, 3, c).start()
 
     def norm_into(ref, base, count):
         @pl.loop(0, count // 16)
@@ -319,64 +325,113 @@
 
     slots = 2 * (nz - 1)
 
-    @pl.loop(0, slots)
-    def _(m):
-        each(1 + m // 2, relay(m % 2))
-
-        @pl.when((m % 2 == 1) & (1 + m // 2 == z) & has_up)
-        def _():
-            for i in range(2):
-                z_copy(2, z, i, True).start()
-
-        @pl.when((m % 2 == 1) & (1 + m // 2 == nz - 1 - z) & has_dn)
-        def _():
-            for i in range(2):
-                z_copy(2, z, i, False).start()
-
-        @pl.when(m >= 2)
-        def _():
-            each(m // 2, diagonal(m % 2))
-
-        @pl.when(m == 0)
-        def _():
-            gate(0)
-
-        @pl.when(m == 1)
-        def _():
-            convolve(0)
-
-    @pl.loop(0, slots)
-    def _(m):
-        t, i = 1 + m // 2, m % 2
-        each(t, onward(i))
-
-        @pl.when(m < 2)
-        def _():
-            each(nz - 1, diagonal(i))
-
-        @pl.when(m == 1)
-        def _():
-            each(1, sideways(0))
-            each(1, sideways(1))
-
-        @pl.when(m >= 2)
-        def _():
-            each(t, sideways(i))
-
-        @pl.when(i == 0)
-        def _():
-            @pl.when(m > 0)
-            def _():
-                convolve(t - 1)
-
-            each(t, finish(0))
-            each(t, finish(1))
-
-        @pl.when(i == 1)
-        def _():
-            gate(t)
-
-    convolve(nz - 1)
+    def own_last(t, i):
+        @pl.when((t == z) & has_up)
+        def _():
+            z_copy(2, z, i, True).start()
+
+        @pl.when((t == nz - 1 - z) & has_dn)
+        def _():
+            z_copy(2, z, i, False).start()
+
+    def at_slot(m, step):
+        each(1 + m // 2, step(m % 2))
+
+    def crossed(t):
+        each(t, relay(2))
+        each(t, sideways(2))
+        own_last(t, 1)
+
+    def over(first, last, body):
+        @pl.loop(first, last)
+        def _(t):
+            body(t)
+
+    at_slot(0, relay)
+    at_slot(0, sideways)
+    gate(0)
+    at_slot(1, relay)
+    at_slot(1, sideways)
+    convolve(0)
+    each(1, relay_far(1))
+    own_last(1, 0)
+    edge = (z == 0) | (z == nz - 1)
+
+    def pairs(t):
+        m = 2 * (t - 1)
+        at_slot(m - 2, diagonal)
+        at_slot(m, relay)
+        at_slot(m, sideways)
+
+        @pl.when(t > 2)
+        def _():
+            at_slot(m - 4, finish)
+            at_slot(m - 3, finish)
+
+    def odds(t):
+        m = 2 * t - 1
+        at_slot(m, relay)
+        at_slot(m - 2, diagonal)
+        at_slot(m, sideways)
+        each(t, relay_far(1))
+        own_last(t, 0)
+
+    def later(t):
+        @pl.when(t > 2)
+        def _():
+            gate(t - 2)
+            convolve(t - 2)
+
+    @pl.when(edge)
+    def _():
+        @pl.loop(2, nz - 1)
+        def _(t):
+            pairs(t)
+            odds(t)
+            later(t)
+
+        pairs(nz - 1)
+        at_slot(slots - 1, relay)
+        at_slot(slots - 3, diagonal)
+        at_slot(slots - 1, sideways)
+        gate(nz - 3)
+        each(nz - 1, relay_far(1))
+        at_slot(slots - 2, diagonal)
+        at_slot(slots - 4, finish)
+        convolve(nz - 3)
+        at_slot(slots - 3, finish)
+        crossed(1)
+        gate(nz - 2)
+        crossed(2)
+        at_slot(slots - 1, diagonal)
+        convolve(nz - 2)
+        at_slot(slots - 2, finish)
+        over(3, nz, crossed)
+        gate(nz - 1)
+        convolve(nz - 1)
+
+    @pl.when(jnp.logical_not(edge))
+    def _():
+        @pl.loop(2, nz - 1)
+        def _(t):
+            pairs(t)
+            odds(t)
+            later(t)
+
+        at_slot(slots - 4, diagonal)
+        at_slot(slots - 6, finish)
+        crossed(1)
+        at_slot(slots - 5, finish)
+        gate(nz - 3)
+        crossed(2)
+        convolve(nz - 3)
+        over(3, nz, crossed)
+        at_slot(slots - 3, diagonal)
+        at_slot(slots - 4, finish)
+        each(1, relay_far(2))
+        gate(nz - 2)
+        over(2, nz, lambda t: each(t, relay_far(2)))
+        convolve(nz - 2)
 
     channels = nz * block
 
@@ -392,23 +447,30 @@
             u = (v - mean) * scale * lng_ref[:, lane] + lnb_ref[:, lane]
             act[i, here, :] = (u * jax.nn.sigmoid(u)).astype(BF16)
 
-    @pl.loop(0, 4)
-    def _(n):
-        @pl.when(n == 2)
-        def _():
-            @pl.loop(1, nz)
-            def _(t):
-                each(t, arrived)
-
-        @pl.loop(0, nz)
-        def _(src):
-            p_copy(src, n, 1 - c).wait_recv()
-
-        here = cols(p_cols(n), quarter)
-        total = x_ref[:, here].astype(F32)
-        for i in range(nz):
-            total = total + jnp.dot(act[i], held[2, i, :, here], preferred_element_type=F32)
-        out_ref[:, here] = total.astype(BF16)
+    def project(t, first):
+        def body(side, src):
+            for n in range(4):
+                p_copy(src, n, 1 - c).wait_recv()
+                here = cols(p_cols(n), quarter)
+                before = x_ref[:, here].astype(F32) if first else acc[n]
+                acc[n] = before + jnp.dot(act[src], held[2, src, :, here], preferred_element_type=F32)
+
+        on_planes(t, body)
+
+    def gather(t):
+        @pl.when(edge)
+        def _():
+            each(t, relay_far(2))
+
+        each(t, diagonal(2))
+
+    gather(1)
+    project(0, True)
+
+    @pl.loop(1, nz - 2)
+    def _(t):
+        gather(t + 1)
+        project(t, False)
 
     @pl.when(has_next)
     def _():
@@ -417,26 +479,52 @@
     for kind in range(3):
         @pl.loop(0, nz)
         def _(src):
-            if final(kind):
-                for slot in range(4):
-                    p_copy(src, slot, c).wait_send()
-            else:
-                d_copy(kind, src, c).wait_send()
-
-            @pl.when(src != z)
-            def _():
-                for i in range(2 if kind < 2 else 1):
-                    x_copy(kind, src, i, False).wait_send()
-                    y_copy(kind, src, i, False).wait_send()
-
-            for i in range(z_pieces(kind)):
-                @pl.when((src <= z) & has_up)
+            far, whole = direct(kind, src), full(kind, src)
+
+            @pl.when((src != z) & jnp.logical_not(whole))
+            def _():
+                x_copy(kind, src, 0, False).wait_send()
+                y_copy(kind, src, 0, False).wait_send()
+
+            @pl.when((src != z) & jnp.logical_not(far | whole))
+            def _():
+                x_copy(kind, src, 1, False).wait_send()
+                y_copy(kind, src, 1, False).wait_send()
+
+            for i in range(4 if kind == 0 else 2):
+                goes = (i == 0) | far if kind else (i == 0) | ((src == z) & edge)
+
+                @pl.when((src <= z) & has_up & goes)
                 def _():
                     z_copy(kind, src, i, True).wait_send()
 
-                @pl.when((src >= z) & has_dn)
+                @pl.when((src >= z) & has_dn & goes)
                 def _():
                     z_copy(kind, src, i, False).wait_send()
+
+    @pl.when(edge)
+    def _():
+        each(nz - 1, relay_far(2))
+
+    project(nz - 2, False)
+    each(nz - 1, diagonal(2))
+
+    for n in (0, 3, 1, 2):
+        here = cols(p_cols(n), quarter)
+        src = nz - 1 - z
+
+        @pl.when(edge)
+        def _():
+            p_copy(src, n, 1 - c).wait_recv()
+            last = jnp.dot(act[src], held[2, src, :, here], preferred_element_type=F32)
+            out_ref[:, here] = (acc[n] + last).astype(BF16)
+
+        @pl.when(jnp.logical_not(edge))
+        def _():
+            out_ref[:, here] = acc[n].astype(BF16)
+
+    sent = held.at[:, :, pl.ds(pl.multiple_of(c * shard, 16), shard)]
+    send(sent, d_send, d_recv.at[0, 0], twin).wait_send()
 
 
 def local(nsp, ntp, stream, norm_gain, w_lin, w_gate, conv_taps, conv_bias, ln_gain, ln_shift, w_proj):
@@ -466,9 +554,10 @@
             pltpu.VMEM((nz, rows, block), F32),
             pltpu.VMEM((nz, rows, block), BF16),
             pltpu.VMEM((nz, kw + 1, block), F32),
+            pltpu.VMEM((4, rows, width // 4), F32),
             dma((9,)), dma((2,)),
-            dma((3, nz, 2)), dma((3, nz, 2)), dma((3, nz, 2)), dma((3, nz)),
-            dma((3, nz, 2)), dma((3, nz, 2)), dma((3, nz, 2)), dma((3, nz, 2)), dma((3, nz)), dma((nz, 4)), dma((nz, 4)),
+            dma((3, nz, 4)), dma((3, nz, 2)), dma((3, nz, 2)), dma((3, nz)),
+            dma((3, nz, 4)), dma((3, nz, 4)), dma((3, nz, 2)), dma((3, nz, 2)), dma, dma((nz, 4)),
         ],
         compiler_params=pltpu.CompilerParams(
             collective_id=0, has_side_effects=True, vmem_limit_bytes=60 * 1024 * 1024

time: 57.5 us -> 51.3 us (0.89)
  Pallas kernels: 56.2 us -> 50 us
    pallas_call x1, Pallas kernels: 56.2 us -> 50 us  [local(): pl.pallas_call(functools.partial(kernel, nsp, nz, kw), out_shape=pltpu.VM...]
where the time goes in v2:
time: 51.3 us; the launch traced here: 51.2 us
  Pallas kernels  50 us (97%)
  local copies, waits for them, and re-layouts  1.15 us (2%)
    pallas_call x1, Pallas kernels, local(): pl.pallas_call(functools.partial(kernel, nsp, nz, kw), out_shape=pltpu.VM...  50 us
    unnamed x1, local copies, waits for them, and re-layouts  1.15 us

profile of v2, /device:TPU:0, one launch (start us, length us, event | category | flops | bytes accessed | tf_op | source)
XLA Modules:
  0.0 51.2 jit_solution(12823563351639174068)
XLA Ops:
  0.0 50.0 %shard_map.91 = bf16[384,2048]{1,0:T(8,128)(2,1)S(1)} custom-call(bf16[384,2048]{1,0:T(8,128)(2,1)} %bitcast.7, f32[1,2048]{1,0:T(1,128)} %bitcast.8, bf16[128,2048]{1,0:T(8,128)(2,1)} %wl_ref.1, bf16[128,2048]{1,0:T(8,128)(2,1)} %wg_ref.1, bf16[128,2048]{1,0:T(8,128)(2,1)} %wp_ref.1, bf16[31,1024]{1,0:T(8,128)(2,1)} %taps_any.1, f32[1,1024]{1,0:T(1,128)} %bitcast.9, ...), custom_call_target="tpu_custom_call" | custom-call | tf_op jit(solution)/shard_map/pallas_call | solution.py:538
  50.0 1.1 %copy.11 = bf16[1,384,2048]{2,1,0:T(8,128)(2,1)} copy(bf16[1,384,2048]{2,1,0:T(8,128)(2,1)S(1)} %bitcast.6) | data formatting | bytes 3145728

commit v3 on v2

--- a/solution.py
+++ b/solution.py
@@ -18,8 +18,8 @@
     nsp, nz, kw,
     x_any, gain_any, wl_ref, wg_ref, wp_ref, taps_any, bias_any, lng_any, lnb_any,
     out_ref,
-    x_ref, gain_ref, taps_ref, bias_ref, lng_ref, lnb_ref, held, xh, normed, mix, conv, act, taps, acc,
-    local_sem, halo_sem, z_recv, x_recv, y_recv, d_recv, up_send, dn_send, x_send, y_send, d_send, dp_recv,
+    x_ref, gain_ref, taps_ref, bias_ref, lng_ref, lnb_ref, held, xh, normed, mix, conv, act, taps, acc, stat, power,
+    local_sem, halo_sem, z_recv, z_first, z_rest, side_recv, corner_recv, d_recv, dp_recv, sent, d_send,
 ):
     rows, width = x_ref.shape
     block = held.shape[2]
@@ -39,6 +39,7 @@
     below = (p, tp - 2)
     has_up, has_dn = z < nz - 1, z > 0
     has_next, has_prev = p < nsp - 1, p > 0
+    edge = (z == 0) | (z == nz - 1)
     qx, qy, qd = q + 1 - 2 * low, q + 2 - 4 * high, 3 - q
 
     def cols(start, size):
@@ -52,6 +53,9 @@
             src_ref=piece, dst_ref=piece, send_sem=ssem, recv_sem=rsem, device_id=target, device_id_type=MESH
         )
 
+    def is_out(kind):
+        return isinstance(kind, int) and kind == 2
+
     def direct(kind, src):
         return (kind == 2) | ((kind == 1) & ((src == 0) | (src == nz - 1)))
 
@@ -59,42 +63,60 @@
         return (kind == 0) & (((src == 0) & (z == 1)) | ((src == nz - 1) & (z == nz - 2)))
 
     def z_copy(kind, src, i, up):
+        if isinstance(kind, int) and kind == 0 and i:
+            arrived = z_rest
+        else:
+            arrived = z_recv.at[src, kind + i + (1 if is_out(kind) else 0)]
         return send(
-            at(kind, src, c, (q, qd, qx, qy)[i] * quarter, quarter),
-            (up_send if up else dn_send).at[kind, src, i], z_recv.at[kind, src, i], above if up else below,
+            at(kind, src, c, (q, qd, qx, qy)[i] * quarter, quarter), sent.at[kind, src], arrived,
+            above if up else below,
         )
 
-    def x_copy(kind, src, i, incoming):
-        if i == 0:
-            piece = at(kind, src, c, (qx if incoming else q) * quarter, quarter)
-        else:
-            piece = at(kind, src, c, (qd if incoming else qy) * quarter, half)
-        return send(piece, x_send.at[kind, src, i], x_recv.at[kind, src, i], beside)
-
-    def y_copy(kind, src, i, incoming):
-        if i == 0:
-            piece = at(kind, src, c, (qy if incoming else q) * quarter, quarter)
-        else:
-            piece = at(kind, src, c, (qd if incoming else qx) * quarter + half, half)
-        return send(piece, y_send.at[kind, src, i], y_recv.at[kind, src, i], across)
-
-    def d_copy(kind, src, core):
-        return send(at(kind, src, core, 0, width), d_send, d_recv.at[kind, src], twin)
+    def part(ref, h):
+        return ref.at[pl.ds(h * (shard // 2), shard // 2)]
+
+    def first_copy(src, h, up, target, arrived):
+        return send(part(at(0, src, c, q * quarter, quarter), h), sent.at[0, src], arrived, target)
+
+    def x_copy(kind, src, i):
+        piece = at(kind, src, c, q * quarter, quarter) if i == 0 else at(kind, src, c, qy * quarter, half)
+        return send(piece, sent.at[kind, src], (corner_recv if i else side_recv).at[kind, src], beside)
+
+    def y_copy(kind, src, i):
+        piece = at(kind, src, c, q * quarter, quarter) if i == 0 else at(kind, src, c, qx * quarter + half, half)
+        return send(piece, sent.at[kind, src], (corner_recv if i else side_recv).at[kind, src], across)
+
+    def landed(kind, src, core, size, arrived):
+        send(at(kind, src, core, 0, size), d_send, arrived, twin).wait_recv()
 
     def d_piece(kind, src, start, size):
-        return send(at(kind, src, c, start, size), d_send, d_recv.at[kind, src], twin)
+        return send(at(kind, src, c, start, size), d_send, d_recv.at[src], twin)
+
+    def is_last(src):
+        return edge & (src == nz - 1 - z)
 
     def p_cols(slot):
         return (q, qx, qy, qd)[slot] * quarter
 
-    def p_copy(src, slot, core):
-        return send(at(2, src, core, p_cols(slot), quarter), d_send, dp_recv.at[src, slot], twin)
+    def p_copy(src, slot):
+        place = jnp.where(is_last(src), nz + slot, src)
+        return send(at(2, src, c, p_cols(slot), quarter), d_send, dp_recv.at[place], twin)
 
     def halo_copy():
         return pltpu.make_async_remote_copy(
             src_ref=x_ref.at[pl.ds(rows - HALO, HALO)], dst_ref=xh, send_sem=halo_sem.at[0],
             recv_sem=halo_sem.at[1], device_id=(p + 1, tp), device_id_type=MESH,
         )
+
+    barrier = pltpu.get_barrier_semaphore()
+    for target in (beside, across, twin):
+        pl.semaphore_signal(barrier, inc=1, device_id=target, device_id_type=MESH)
+    for there, target in (
+        (has_up, above), (has_dn, below), (has_next, (p + 1, tp)), (has_prev, (p - 1, tp)),
+    ):
+        @pl.when(there)
+        def _():
+            pl.semaphore_signal(barrier, inc=1, device_id=target, device_id_type=MESH)
 
     mine = [
         pltpu.make_async_copy(ref, at(kind, z, c, 0, width), local_sem.at[kind])
@@ -114,16 +136,6 @@
         copy.start()
     mine[2].start()
 
-    barrier = pltpu.get_barrier_semaphore()
-    for target in (beside, across, twin):
-        pl.semaphore_signal(barrier, inc=1, device_id=target, device_id_type=MESH)
-    for there, target in (
-        (has_up, above), (has_dn, below), (has_next, (p + 1, tp)), (has_prev, (p - 1, tp)),
-    ):
-        @pl.when(there)
-        def _():
-            pl.semaphore_signal(barrier, inc=1, device_id=target, device_id_type=MESH)
-
     one = lambda there: jnp.where(there, 1, 0)
     pl.semaphore_wait(barrier, 3 + one(has_up) + one(has_dn) + one(has_next) + one(has_prev))
 
@@ -140,8 +152,12 @@
                     z_copy(kind, z, i, up).start()
 
     mine[0].wait()
-    start_own(0, 0, True)
-    start_own(0, 0, False)
+    for h in range(2):
+        for up, there in ((True, has_up), (False, has_dn)):
+            @pl.when(there)
+            def _():
+                first_copy(z, h, up, above if up else below, z_first.at[0 if up else 1, h]).start()
+
     mine[1].wait()
     start_own(1, 0, True)
     start_own(1, 0, False)
@@ -152,11 +168,11 @@
     def _():
         halo_copy().start()
 
-    d_copy(0, z, c).start()
-    d_copy(1, z, c).start()
+    d_piece(0, z, 0, width).start()
+    d_piece(1, z, 0, width).start()
     mine[2].wait()
     for slot in range(4):
-        p_copy(z, slot, c).start()
+        p_copy(z, slot).start()
 
     start_ends((2, 0), (2, 1))
 
@@ -180,8 +196,8 @@
                 z_copy(kind, src, i, False).start()
 
     def twin_piece(kind, src, slot):
-        if isinstance(kind, int) and kind == 2:
-            p_copy(src, slot, c).start()
+        if is_out(kind):
+            p_copy(src, slot).start()
         else:
             d_piece(kind, src, p_cols(slot), quarter).start()
 
@@ -189,8 +205,8 @@
         def body(src, sign):
             @pl.when(jnp.logical_not(full(kind, src)))
             def _():
-                x_copy(kind, src, 0, False).start()
-                y_copy(kind, src, 0, False).start()
+                x_copy(kind, src, 0).start()
+                y_copy(kind, src, 0).start()
 
         return body
 
@@ -210,25 +226,35 @@
 
         return body
 
+    def first_relay(src, sign):
+        for h in range(2):
+            first_copy(src, h, True, above, z_first.at[0 if sign < 0 else 1, h]).wait_recv()
+            onward, target = (has_up, above) if sign < 0 else (has_dn, below)
+
+            @pl.when(onward)
+            def _():
+                first_copy(src, h, True, target, z_recv.at[src, 0]).start()
+
+            @pl.when(jnp.logical_not(full(0, src)))
+            def _():
+                for target in (beside, across):
+                    first_copy(src, h, True, target, side_recv.at[0, src]).start()
+
+            send(part(at(0, src, c, q * quarter, quarter), h), d_send, d_recv.at[src], twin).start()
+
     def diagonal(kind):
         def body(src, sign):
-            more = jnp.logical_not(direct(kind, src))
-
             @pl.when(jnp.logical_not(full(kind, src)))
             def _():
-                x_copy(kind, src, 0, True).wait_recv()
-
-                @pl.when(more)
-                def _():
-                    y_copy(kind, src, 1, False).start()
+                landed(kind, src, c, 2 * quarter, side_recv.at[kind, src])
+
+                if not is_out(kind):
+                    @pl.when(jnp.logical_not(direct(kind, src)))
+                    def _():
+                        y_copy(kind, src, 1).start()
+                        x_copy(kind, src, 1).start()
 
                 twin_piece(kind, src, 1)
-                y_copy(kind, src, 0, True).wait_recv()
-
-                @pl.when(more)
-                def _():
-                    x_copy(kind, src, 1, False).start()
-
                 twin_piece(kind, src, 2)
 
         return body
@@ -239,28 +265,45 @@
 
             @pl.when(jnp.logical_not(direct(kind, src) | whole))
             def _():
-                x_copy(kind, src, 1, True).wait_recv()
-                d_piece(kind, src, qd * quarter, half).start()
-                y_copy(kind, src, 1, True).wait_recv()
-                d_piece(kind, src, qd * quarter + half, half).start()
+                landed(kind, src, c, quarter, corner_recv.at[kind, src])
+                twin_piece(kind, src, 3)
 
             @pl.when(whole)
             def _():
-                for i, slot in ((1, 3), (2, 1), (3, 2)):
-                    z_copy(kind, src, i, True).wait_recv()
+                landed(kind, src, c, 3 * quarter, z_rest)
+                for slot in range(1, 4):
                     twin_piece(kind, src, slot)
 
         return body
 
     def norm_into(ref, base, count):
+        spans = [slice(i * 128, (i + 1) * 128) for i in range(width // 128)]
+
+        def there(r):
+            return pl.ds(pl.multiple_of(base + r * 16, 16), 16)
+
         @pl.loop(0, count // 16)
         def _(r):
-            full = ref[pl.ds(pl.multiple_of(r * 16, 16), 16), :].astype(F32)
-            scale = lax.rsqrt(jnp.mean(full * full, axis=1, keepdims=True) + EPS)
-            normed[pl.ds(pl.multiple_of(base + r * 16, 16), 16), :] = (full * scale * gain_ref[...]).astype(BF16)
+            total = jnp.zeros((16, 128), F32)
+            for span in spans:
+                full = ref[pl.ds(pl.multiple_of(r * 16, 16), 16), span].astype(F32)
+                total = total + full * full
+            power[there(r), :] = total
+
+        whole = slice(base, base + count)
+        mean = jnp.sum(power[whole, :], axis=1, keepdims=True) / width
+        power[whole, :] = jnp.broadcast_to(lax.rsqrt(mean + EPS), (count, 128))
+
+        @pl.loop(0, count // 16)
+        def _(r):
+            scale = power[there(r), :]
+            for span in spans:
+                full = ref[pl.ds(pl.multiple_of(r * 16, 16), 16), span].astype(F32)
+                normed[there(r), span] = (full * scale * gain_ref[:, span]).astype(BF16)
 
     for copy in small:
         copy.wait()
+    stat[...] = jnp.zeros_like(stat)
     norm_into(x_ref, HALO, rows)
     for i in range(nz):
         taps[i, 0:kw] = taps_ref[:, i * block:(i + 1) * block].astype(F32)
@@ -295,8 +338,8 @@
 
     def gate(t):
         def body(side, src):
-            d_copy(0, src, 1 - c).wait_recv()
-            d_copy(1, src, 1 - c).wait_recv()
+            pair = held.at[0:2, src, pl.ds(pl.multiple_of((1 - c) * shard, 16), shard)]
+            send(pair, d_send, d_recv.at[src], twin).wait_recv()
             linear = lax.dot_general(normed[...], held[0, src], nt, preferred_element_type=F32)
             gating = lax.dot_general(normed[...], held[1, src], nt, preferred_element_type=F32)
             mixed = (linear * jax.nn.sigmoid(gating)).astype(BF16).astype(F32)
@@ -310,6 +353,7 @@
             @pl.loop(0, rows // tile)
             def _(r):
                 base = pl.multiple_of(r * tile, tile)
+                line, square = stat[0, pl.ds(base, tile), :], stat[1, pl.ds(base, tile), :]
                 for s in range(strips):
                     lane = slice(s * lanes, (s + 1) * lanes)
                     total = jnp.broadcast_to(taps[src, kw:kw + 1, lane], (tile, lanes))
@@ -320,6 +364,10 @@
                             if 0 <= tap < kw:
                                 total = total + taps[src, tap:tap + 1, lane] * slab[8 * a:8 * a + tile]
                     conv[src, pl.ds(base, tile), lane] = total
+                    line = line + total
+                    square = square + total * total
+                stat[0, pl.ds(base, tile), :] = line
+                stat[1, pl.ds(base, tile), :] = square
 
         on_planes(t, body)
 
@@ -347,15 +395,13 @@
         def _(t):
             body(t)
 
-    at_slot(0, relay)
-    at_slot(0, sideways)
+    each(1, first_relay)
     gate(0)
     at_slot(1, relay)
     at_slot(1, sideways)
     convolve(0)
     each(1, relay_far(1))
     own_last(1, 0)
-    edge = (z == 0) | (z == nz - 1)
 
     def pairs(t):
         m = 2 * (t - 1)
@@ -401,8 +447,8 @@
         convolve(nz - 3)
         at_slot(slots - 3, finish)
         crossed(1)
+        crossed(2)
         gate(nz - 2)
-        crossed(2)
         at_slot(slots - 1, diagonal)
         convolve(nz - 2)
         at_slot(slots - 2, finish)
@@ -434,28 +480,34 @@
         convolve(nz - 2)
 
     channels = nz * block
+    mean = jnp.sum(stat[0], axis=1, keepdims=True) / channels
+    meansq = jnp.sum(stat[1], axis=1, keepdims=True) / channels
+    stat[0] = jnp.broadcast_to(mean, stat.shape[1:])
+    stat[1] = jnp.broadcast_to(lax.rsqrt(meansq - mean * mean + EPS), stat.shape[1:])
 
     @pl.loop(0, rows // 16)
     def _(r):
         here = pl.ds(pl.multiple_of(r * 16, 16), 16)
-        parts = [conv[i, here, :] for i in range(nz)]
-        mean = sum(jnp.sum(v, axis=1, keepdims=True) for v in parts) / channels
-        meansq = sum(jnp.sum(v * v, axis=1, keepdims=True) for v in parts) / channels
-        scale = lax.rsqrt(meansq - mean * mean + EPS)
-        for i, v in enumerate(parts):
-            lane = slice(i * block, (i + 1) * block)
-            u = (v - mean) * scale * lng_ref[:, lane] + lnb_ref[:, lane]
-            act[i, here, :] = (u * jax.nn.sigmoid(u)).astype(BF16)
-
-    def project(t, first):
-        def body(side, src):
-            for n in range(4):
-                p_copy(src, n, 1 - c).wait_recv()
-                here = cols(p_cols(n), quarter)
-                before = x_ref[:, here].astype(F32) if first else acc[n]
-                acc[n] = before + jnp.dot(act[src], held[2, src, :, here], preferred_element_type=F32)
-
-        on_planes(t, body)
+        for i in range(nz):
+            for s in range(strips):
+                lane = slice(s * lanes, (s + 1) * lanes)
+                both = slice(i * block + s * lanes, i * block + (s + 1) * lanes)
+                u = (conv[i, here, lane] - stat[0, here, :]) * stat[1, here, :] * lng_ref[:, both] + lnb_ref[:, both]
+                act[i, here, lane] = (u * jax.nn.sigmoid(u)).astype(BF16)
+
+    def ready(src):
+        landed(2, src, 1 - c, width, dp_recv.at[src])
+
+    def products(srcs, here):
+        return sum(jnp.dot(act[src], held[2, src, :, here], preferred_element_type=F32) for src in srcs)
+
+    def project(srcs, first):
+        for src in srcs:
+            ready(src)
+        for n in range(4):
+            here = cols(p_cols(n), quarter)
+            before = x_ref[:, here].astype(F32) if first else acc[n]
+            acc[n] = before + products(srcs, here)
 
     def gather(t):
         @pl.when(edge)
@@ -464,67 +516,87 @@
 
         each(t, diagonal(2))
 
-    gather(1)
-    project(0, True)
-
-    @pl.loop(1, nz - 2)
-    def _(t):
-        gather(t + 1)
-        project(t, False)
-
-    @pl.when(has_next)
-    def _():
-        halo_copy().wait_send()
-
-    for kind in range(3):
+    def drain(kind):
         @pl.loop(0, nz)
         def _(src):
-            far, whole = direct(kind, src), full(kind, src)
-
-            @pl.when((src != z) & jnp.logical_not(whole))
-            def _():
-                x_copy(kind, src, 0, False).wait_send()
-                y_copy(kind, src, 0, False).wait_send()
-
-            @pl.when((src != z) & jnp.logical_not(far | whole))
-            def _():
-                x_copy(kind, src, 1, False).wait_send()
-                y_copy(kind, src, 1, False).wait_send()
-
-            for i in range(4 if kind == 0 else 2):
-                goes = (i == 0) | far if kind else (i == 0) | ((src == z) & edge)
-
-                @pl.when((src <= z) & has_up & goes)
+            far, own, passed = direct(kind, src) * 1, (src == z), ((src < z) & has_up) | ((src > z) & has_dn)
+            other = jnp.where(full(kind, src), 0, 3 - far) + passed * (1 + far)
+            mine = edge * (4, 2, 2)[kind] + (1 - edge * 1) * 2 * (1, 1, 2)[kind]
+            count = jnp.where(own, mine, other)
+            for n in range(1, 5):
+                @pl.when(count == n)
                 def _():
-                    z_copy(kind, src, i, True).wait_send()
-
-                @pl.when((src >= z) & has_dn & goes)
-                def _():
-                    z_copy(kind, src, i, False).wait_send()
+                    send(at(kind, src, c, 0, n * quarter), sent.at[kind, src], d_send, twin).wait_send()
+
+    def inward(t):
+        return jnp.where(z == 0, t, nz - 1 - t)
+
+    near_edge = (z == 1) | (z == nz - 2)
+    beyond = jnp.where(z == 1, nz - 1, 0)
+
+    def finalize(srcs, n):
+        here = cols(p_cols(n), quarter)
+        out_ref[:, here] = (acc[n] + products(srcs, here)).astype(BF16) if srcs else acc[n].astype(BF16)
+
+    gather(1)
+    if nz == 4:
+        gather(2)
 
     @pl.when(edge)
     def _():
+        project([z, inward(1)], True)
+
+    @pl.when(jnp.logical_not(edge))
+    def _():
+        project([z, z - 1, z + 1], True)
+
+    drain(0)
+    drain(1)
+
+    @pl.loop(2, nz - 2)
+    def _(t):
+        gather(t)
+        each(t, lambda src, sign: project([src], False))
+
+    if nz > 4:
+        gather(nz - 2)
+
+    @pl.when(edge)
+    def _():
+        lasts = [inward(nz - 2), inward(nz - 1)]
+
+        def complete(n):
+            landed(2, inward(nz - 1), 1 - c, quarter, dp_recv.at[nz + n])
+            finalize(lasts, n)
+
         each(nz - 1, relay_far(2))
-
-    project(nz - 2, False)
-    each(nz - 1, diagonal(2))
-
-    for n in (0, 3, 1, 2):
-        here = cols(p_cols(n), quarter)
-        src = nz - 1 - z
-
-        @pl.when(edge)
-        def _():
-            p_copy(src, n, 1 - c).wait_recv()
-            last = jnp.dot(act[src], held[2, src, :, here], preferred_element_type=F32)
-            out_ref[:, here] = (acc[n] + last).astype(BF16)
-
-        @pl.when(jnp.logical_not(edge))
-        def _():
-            out_ref[:, here] = acc[n].astype(BF16)
-
-    sent = held.at[:, :, pl.ds(pl.multiple_of(c * shard, 16), shard)]
-    send(sent, d_send, d_recv.at[0, 0], twin).wait_send()
+        ready(inward(nz - 2))
+        complete(0)
+        each(nz - 1, diagonal(2))
+        complete(3)
+        complete(1)
+        complete(2)
+
+    @pl.when(near_edge)
+    def _():
+        ready(beyond)
+        for n in range(4):
+            finalize([beyond], n)
+
+    if nz > 4:
+        @pl.when(jnp.logical_not(edge | near_edge))
+        def _():
+            for n in range(4):
+                finalize([], n)
+
+    drain(2)
+
+    @pl.when(has_next)
+    def _():
+        halo_copy().wait_send()
+
+    passed_on = held.at[:, :, pl.ds(pl.multiple_of(c * shard, 16), shard)]
+    send(passed_on, d_send, d_recv.at[0], twin).wait_send()
 
 
 def local(nsp, ntp, stream, norm_gain, w_lin, w_gate, conv_taps, conv_bias, ln_gain, ln_shift, w_proj):
@@ -555,9 +627,10 @@
             pltpu.VMEM((nz, rows, block), BF16),
             pltpu.VMEM((nz, kw + 1, block), F32),
             pltpu.VMEM((4, rows, width // 4), F32),
+            pltpu.VMEM((2, rows, lanes), F32),
+            pltpu.VMEM((HALO + rows, 128), F32),
             dma((9,)), dma((2,)),
-            dma((3, nz, 4)), dma((3, nz, 2)), dma((3, nz, 2)), dma((3, nz)),
-            dma((3, nz, 4)), dma((3, nz, 4)), dma((3, nz, 2)), dma((3, nz, 2)), dma, dma((nz, 4)),
+            dma((nz, 5)), dma((2, 2)), dma, dma((3, nz)), dma((2, nz)), dma((nz,)), dma((nz + 4,)), dma((3, nz)), dma,
         ],
         compiler_params=pltpu.CompilerParams(
             collective_id=0, has_side_effects=True, vmem_limit_bytes=60 * 1024 * 1024

time: 51.3 us -> 46.9 us (0.914)
  Pallas kernels: 50 us -> 45.3 us
    pallas_call x1, Pallas kernels: 50 us -> 45.3 us  [local(): pl.pallas_call(functools.partial(kernel, nsp, nz, kw), out_shape=pltpu.VM...]
where the time goes in v3:
time: 46.9 us; the launch traced here: 46.4 us
  Pallas kernels  45.3 us (97%)
  local copies, waits for them, and re-layouts  1.15 us (2%)
    pallas_call x1, Pallas kernels, local(): pl.pallas_call(functools.partial(kernel, nsp, nz, kw), out_shape=pltpu.VM...  45.3 us
    unnamed x1, local copies, waits for them, and re-layouts  1.15 us

profile of v3, /device:TPU:0, one launch (start us, length us, event | category | flops | bytes accessed | tf_op | source)
XLA Modules:
  0.0 46.4 jit_solution(13262970213330488245)
XLA Ops:
  0.0 45.3 %shard_map.91 = bf16[384,2048]{1,0:T(8,128)(2,1)S(1)} custom-call(bf16[384,2048]{1,0:T(8,128)(2,1)} %bitcast.7, f32[1,2048]{1,0:T(1,128)} %bitcast.8, bf16[128,2048]{1,0:T(8,128)(2,1)} %wl_ref.1, bf16[128,2048]{1,0:T(8,128)(2,1)} %wg_ref.1, bf16[128,2048]{1,0:T(8,128)(2,1)} %wp_ref.1, bf16[31,1024]{1,0:T(8,128)(2,1)} %taps_any.1, f32[1,1024]{1,0:T(1,128)} %bitcast.9, ...), custom_call_target="tpu_custom_call" | custom-call | tf_op jit(solution)/shard_map/pallas_call | solution.py:610
  45.3 1.1 %copy.11 = bf16[1,384,2048]{2,1,0:T(8,128)(2,1)} copy(bf16[1,384,2048]{2,1,0:T(8,128)(2,1)S(1)} %bitcast.6) | data formatting | bytes 3145728
